TPU v7x, 32 devices: a whole 2x2x4 slice. The times are simulated.
32 devices in a mesh: kv: 8 (over z, y), tp: 4 (over x, core).
Axes of the slice: x: 2, y: 2, z: 4, core: 2. Of those that a mesh axis runs over, the one named last changes fastest.
Arguments:
- tokens: bfloat16 [16, 4, 4096], P(None, None, 'kv'), may hold values from -20 to 20
- mix_gain: float32 [4096], P('kv'), may hold values from 0.1 to 1.9
- w_query: bfloat16 [4096, 2048], P('kv', 'tp'), may hold values from -0.09375 to 0.09375
- w_key: bfloat16 [4096, 2048], P('kv', 'tp'), may hold values from -0.09375 to 0.09375
- w_value: bfloat16 [4096, 2048], P('kv', 'tp'), may hold values from -0.09375 to 0.09375
- w_forget: bfloat16 [4096, 16], replicated, may hold values from -0.09375 to 0.09375
- forget_bias: float32 [16], P('tp'), may hold values from -1 to 3
- key_cache: bfloat16 [16, 4096, 2048], P(None, 'kv', 'tp'), may hold values from -6 to 6
- value_cache: bfloat16 [16, 4096, 2048], P(None, 'kv', 'tp'), may hold values from -6 to 6
- cum_gate: float32 [16, 16, 4096], P(None, 'tp', 'kv'), may hold values from -761.52 to 0, as said below
- lengths: int32 [16], replicated, may hold values from 1 to 4096, 16381 in all
- w_out: bfloat16 [2048, 4096], P('tp', 'kv'), may hold values from -0.125 to 0.125
- mlp_gain: float32 [4096], P('kv'), may hold values from 0.1 to 1.9
- w_gate: bfloat16 [4096, 11264], P('kv', 'tp'), may hold values from -0.09375 to 0.09375
- w_up: bfloat16 [4096, 11264], P('kv', 'tp'), may hold values from -0.09375 to 0.09375
- w_down: bfloat16 [11264, 4096], P('tp', 'kv'), may hold values from -0.0546875 to 0.0546875
Outputs:
- result: bfloat16 [16, 4, 4096], P(None, None, 'kv')
Inputs may be any that keep to these rules, and one draw needn't show every extreme that they name: `cum_gate`: never rising along positions. `lengths`: one sequence fills all 4096 positions.
All inputs are finite; a program needn't handle non-finite values.
Results may differ from a plain program's by a relative error of at most 0.02.
Values may be sent and summed in bfloat16 or wider, within the bound.
A program may use at most 64 MiB of HBM per device.

v0:
```python
import jax
import jax.numpy as jnp
from jax import lax
from jax.sharding import PartitionSpec as P

D = 4096


EPSILON = 1e-06
NEG_FILL = -1e30


def combined_all(array, axis, combine):
    everything = jax.tree.map(lambda part: lax.all_gather(part, axis), array)
    first = jax.tree.map(lambda part: part[0], everything)

    def turn(k, so_far):
        return combine(so_far, jax.tree.map(lambda part: part[k], everything))

    return lax.fori_loop(1, lax.axis_size(axis), turn, first)


def on_device(
    tokens,
    mix_gain,
    w_query,
    w_key,
    w_value,
    w_forget,
    forget_bias,
    key_cache,
    value_cache,
    cum_gate,
    lengths,
    w_out,
    mlp_gain,
    w_gate,
    w_up,
    w_down,
):
    seq_count, new_count, local_width = tokens.shape
    row_count = seq_count * new_count
    heads_dev = forget_bias.shape[0]
    head_width = w_query.shape[1] // heads_dev
    pos_dev = key_cache.shape[1]
    kv_index = lax.axis_index("kv")
    tp_index = lax.axis_index("tp")
    inputs = tokens.reshape(row_count, local_width).astype(jnp.float32)
    scaled = (inputs * mix_gain).astype(jnp.bfloat16)
    forget_rows = lax.dynamic_slice_in_dim(w_forget, kv_index * local_width, local_width, 0)
    forget_cols = lax.dynamic_slice_in_dim(forget_rows, tp_index * heads_dev, heads_dev, 1)
    query_part = jnp.dot(scaled, w_query, preferred_element_type=jnp.float32)
    key_part = jnp.dot(scaled, w_key, preferred_element_type=jnp.float32)
    value_part = jnp.dot(scaled, w_value, preferred_element_type=jnp.float32)
    forget_part = jnp.dot(scaled, forget_cols, preferred_element_type=jnp.float32)
    squares = jnp.sum(inputs * inputs, axis=1)
    query_sum, key_sum, value_sum, forget_sum, square_sum = (
        lax.psum(query_part.astype(jnp.bfloat16), "kv").astype(jnp.float32),
        lax.psum(key_part.astype(jnp.bfloat16), "kv").astype(jnp.float32),
        lax.psum(value_part.astype(jnp.bfloat16), "kv").astype(jnp.float32),
        lax.psum(forget_part.astype(jnp.bfloat16), "kv").astype(jnp.float32),
        lax.psum(squares.astype(jnp.bfloat16), "kv").astype(jnp.float32),
    )
    inv_norm = lax.rsqrt(square_sum / D + EPSILON)[:, None]
    head_shape = (seq_count, new_count, heads_dev, head_width)
    query = (inv_norm * query_sum).astype(jnp.bfloat16).reshape(head_shape)
    key_new = (inv_norm * key_sum).astype(jnp.bfloat16).reshape(head_shape)
    value_new = (inv_norm * value_sum).astype(jnp.bfloat16).reshape(head_shape)
    log_forget = jax.nn.log_sigmoid(inv_norm * forget_sum + forget_bias).reshape(
        seq_count, new_count, heads_dev
    )
    score_scale = head_width ** (-0.5)
    positions = kv_index * pos_dev + jnp.arange(pos_dev, dtype=jnp.int32)
    live_rows = positions[None, :] < lengths[:, None]
    live_mask = live_rows[:, None, None, :]
    cached_keys = key_cache.reshape(seq_count, pos_dev, heads_dev, head_width)
    cached_values = value_cache.reshape(seq_count, pos_dev, heads_dev, head_width)
    scores = jnp.einsum("bthd,bphd->bthp", query, cached_keys, preferred_element_type=jnp.float32)
    scores = scores * score_scale - cum_gate[:, None]
    scores = jnp.where(live_mask, scores, NEG_FILL)
    block_peak = jnp.max(scores, axis=3)
    weights = jnp.where(live_mask, jnp.exp(scores - block_peak[..., None]), 0.0)
    block_total = jnp.sum(weights, axis=3)
    block_sum = jnp.einsum(
        "bthp,bphd->bthd",
        weights.astype(jnp.bfloat16),
        cached_values,
        preferred_element_type=jnp.float32,
    )
    last_hit = positions[None, :] == (lengths - 1)[:, None]
    last_piece = jnp.sum(jnp.where(last_hit[:, None, :], cum_gate, 0.0), axis=2)

    def combine(first, second):
        peak_both = jnp.maximum(first[0], second[0])
        first_factor = jnp.exp(first[0] - peak_both)
        second_factor = jnp.exp(second[0] - peak_both)
        return (
            peak_both,
            first[1] * first_factor + second[1] * second_factor,
            first[2] * first_factor[..., None] + second[2] * second_factor[..., None],
            first[3] + second[3],
        )

    past_peak, past_total, past_sum, last_cum = combined_all(
        (block_peak, block_total, block_sum, last_piece), "kv", combine
    )
    key_cum = last_cum[:, None, :] + jnp.cumsum(log_forget, axis=1)
    own_scores = (
        jnp.einsum("bthd,bshd->bths", query, key_new, preferred_element_type=jnp.float32)
        * score_scale
    )
    own_scores = own_scores - jnp.transpose(key_cum, (0, 2, 1))[:, None]
    causal = (jnp.arange(new_count)[:, None] >= jnp.arange(new_count)[None, :])[None, :, None, :]
    own_scores = jnp.where(causal, own_scores, NEG_FILL)
    peak_score = jnp.maximum(past_peak, jnp.max(own_scores, axis=3))
    past_factor = jnp.exp(past_peak - peak_score)
    own_weights = jnp.where(causal, jnp.exp(own_scores - peak_score[..., None]), 0.0)
    numerator = past_sum * past_factor[..., None] + jnp.einsum(
        "bths,bshd->bthd",
        own_weights.astype(jnp.bfloat16),
        value_new,
        preferred_element_type=jnp.float32,
    )
    denominator = past_total * past_factor + jnp.sum(own_weights, axis=3)
    attended = (
        (numerator / denominator[..., None])
        .astype(jnp.bfloat16)
        .reshape(row_count, heads_dev * head_width)
    )
    attn_out = lax.psum(
        jnp.dot(attended, w_out, preferred_element_type=jnp.float32).astype(jnp.bfloat16), "tp"
    ).astype(jnp.float32)
    middle = (inputs + attn_out).astype(jnp.bfloat16)
    middle_wide = middle.astype(jnp.float32)
    squares2 = jnp.sum(middle_wide * middle_wide, axis=1)
    scaled2 = (middle_wide * mlp_gain).astype(jnp.bfloat16)
    gate_part = jnp.dot(scaled2, w_gate, preferred_element_type=jnp.float32)
    up_part = jnp.dot(scaled2, w_up, preferred_element_type=jnp.float32)
    gate_sum, up_sum, square_sum2 = (
        lax.psum(gate_part.astype(jnp.bfloat16), "kv").astype(jnp.float32),
        lax.psum(up_part.astype(jnp.bfloat16), "kv").astype(jnp.float32),
        lax.psum(squares2.astype(jnp.bfloat16), "kv").astype(jnp.float32),
    )
    inv_norm2 = lax.rsqrt(square_sum2 / D + EPSILON)[:, None]
    hidden = (jax.nn.silu(inv_norm2 * gate_sum) * (inv_norm2 * up_sum)).astype(jnp.bfloat16)
    down_part = jnp.dot(hidden, w_down, preferred_element_type=jnp.float32)
    mixed = lax.psum(down_part.astype(jnp.bfloat16), "tp").astype(jnp.float32)
    return (middle_wide + mixed).astype(jnp.bfloat16).reshape(seq_count, new_count, local_width)


def solution(mesh):
    in_specs = (
        P(None, None, "kv"),
        P("kv"),
        P("kv", "tp"),
        P("kv", "tp"),
        P("kv", "tp"),
        P(),
        P("tp"),
        P(None, "kv", "tp"),
        P(None, "kv", "tp"),
        P(None, "tp", "kv"),
        P(),
        P("tp", "kv"),
        P("kv"),
        P("kv", "tp"),
        P("kv", "tp"),
        P("tp", "kv"),
    )
    out_specs = P(None, None, "kv")
    return jax.shard_map(
        on_device, mesh=mesh, in_specs=in_specs, out_specs=out_specs, check_vma=False
    )
```

profile of v0, /device:TPU:0, one launch (start us, length us, event | category | flops | bytes accessed | tf_op | source)
XLA Modules:
  0.0 381.2 jit_solution(16673894785011786111)
XLA Ops:
  8.2 1.9 convolution_convert_fusion.4
  10.1 1.9 convolution_convert_fusion.5
  12.0 1.9 convolution_convert_fusion.6
  15.7 1.3 broadcast_compare_fusion
  17.9 23.7 %all-reduce = (bf16[64]{0:T(256)(128)(2,1)S(1)}, bf16[64,4]{0,1:T(4,128)(2,1)}) all-reduce(bf16[64]{0:T(256)(128)(2,1)S(1)} %convert_element_type.112, bf16[64,4]{0,1:T(4,128)(2,1)S(1)} %convolution_convert_fusion.7), channel_id=1, replica_groups=mesh['kv'=8,'tp'=4] {'kv'}, use_global_device_ids=true, to_apply=%region_1.0 | all-reduce | flops 320 | bytes 1280 | tf_op jit(solution)/shard_map/psum | solution.py:62
  41.7 46.5 %all-reduce.14.cloned.1.call-done = (bf16[64,512]{1,0:T(8,128)(2,1)}, bf16[64,512]{1,0:T(8,128)(2,1)}, bf16[64,512]{1,0:T(8,128)(2,1)}) async-done(((bf16[64,512]{1,0:T(8,128)(2,1)}, bf16[64,512]{1,0:T(8,128)(2,1)}, bf16[64,512]{1,0:T(8,128)(2,1)}), (bf16[64,512]{1,0:T(8,128)(2,1)}, bf16[64,512]{1,0:T(8,128)(2,1)}, bf16[64,512]{1,0:T(8,128)(2,1)})) %all-reduce.14.cloned.1.call-update) | async-done | bytes 196624 | tf_op jit(solution)/shard_map/psum | solution.py:58
  88.1 1.6 multiply_convert_fusion.2
  90.4 5.9 %fusion.55 = (f32[16,4,4]{1,2,0:T(4,128)S(1)}, f32[16,4,4,512]{3,1,2,0:T(4,128)S(1)}) fusion(f32[16,4,512]{2,1,0:T(4,128)} %param.27, bf16[16,4,4,128]{3,2,1,0:T(4,128)(2,1)} %reshape.105, pred[16,512]{1,0:T(8,128)(4,1)S(1)} %get-tuple-element.304, bf16[16,512,512]{2,1,0:T(8,128)(2,1)} %param.25), kind=kOutput, calls=%fused_computation.83 | convolution fusion | flops 34078464 | bytes 9118720 | tf_op jit(solution)/shard_map/bthd,bphd->bthp/dot_general | solution.py:78
  99.0 1.6 select_reduce_fusion
  102.9 2.9 reduce_window_sum.11
  105.7 26.1 %all-gather.4 = f32[8,16,4]{1,2,0:T(4,128)S(1)} all-gather(f32[1,16,4]{1,2,0:T(4,128)S(1)} %bitcast.110), channel_id=5, replica_groups=mesh['kv'=8,'tp'=4] {'kv'}, dimensions={0}, use_global_device_ids=true | all-gather | bytes 2304 | tf_op jit(solution)/shard_map/all_gather | solution.py:14
  132.5 1.5 copy.88
  134.0 1.5 reshape.110
  135.5 1.5 reshape.108
  137.0 1.7 fusion.41
  138.7 1.7 copy.101
  140.4 1.8 fusion.27
  143.1 30.9 %all-gather.1 = f32[128,4,4]{2,1,0:T(4,128)S(1)} all-gather(f32[16,4,4]{2,1,0:T(4,128)S(1)} %copy.89), channel_id=3, replica_groups=mesh['kv'=8,'tp'=4] {'kv'}, dimensions={0}, use_global_device_ids=true | all-gather | bytes 9216 | tf_op jit(solution)/shard_map/all_gather | solution.py:14
  174.4 31.0 %all-gather = f32[128,4,4]{2,1,0:T(4,128)S(1)} all-gather(f32[16,4,4]{2,1,0:T(4,128)} %copy.88), channel_id=2, replica_groups=mesh['kv'=8,'tp'=4] {'kv'}, dimensions={0}, use_global_device_ids=true | all-gather | bytes 9216 | tf_op jit(solution)/shard_map/all_gather | solution.py:14
  206.7 15.8 %while.21 = (s32[]{:T(128)}, f32[16,4,4]{0,2,1:T(4,128)S(1)}, f32[16,4,4]{0,2,1:T(4,128)S(1)}, f32[16,4,4,128]{3,2,1,0:T(4,128)S(1)}, f32[16,4]{0,1:T(4,128)S(1)...) while((s32[]{:T(128)}, f32[16,4,4]{0,2,1:T(4,128)S(1)}, ...), condition=%wide.region_7.8_spmd, body=%wide.region_6.7_spmd.sunk | while | flops 99909 | bytes 408483 | solution.py:20
  207.6 1.3 fusion.73
  209.9 1.3 fusion.73
  212.1 1.3 fusion.73
  221.2 1.3 fusion.73
  226.6 1.9 convolution_convert_fusion.3
  228.6 29.2 %all-reduce.8.cloned.1.call-done = bf16[64,512]{1,0:T(8,128)(2,1)} async-done(((bf16[64,512]{1,0:T(8,128)(2,1)}), bf16[64,512]{1,0:T(8,128)(2,1)}) %all-reduce.8.cloned.1.call-update) | async-done | bytes 65552 | tf_op jit(solution)/shard_map/psum | solution.py:130
  258.8 2.0 convolution_convert_fusion.1
  260.8 3.2 convolution_convert_fusion
  264.1 21.6 %psum.76 = bf16[64]{0:T(256)(128)(2,1)S(1)} all-reduce(bf16[64]{0:T(256)(128)(2,1)S(1)} %get-tuple-element.297), channel_id=1, replica_groups=mesh['kv'=8,'tp'=4] {'kv'}, use_global_device_ids=true, to_apply=%region_16.17 | all-reduce | flops 64 | bytes 256 | tf_op jit(solution)/shard_map/psum | solution.py:142
  285.7 53.3 %all-reduce.12.cloned.1.call-done = (bf16[64,2816]{1,0:T(8,128)(2,1)}, bf16[64,2816]{1,0:T(8,128)(2,1)}) async-done(((bf16[64,2816]{1,0:T(8,128)(2,1)}, bf16[64,2816]{1,0:T(8,128)(2,1)}), (bf16[64,2816]{1,0:T(8,128)(2,1)}, bf16[64,2816]{1,0:T(8,128)(2,1)})) %all-reduce.12.cloned.1.call-update) | async-done | bytes 720912 | tf_op jit(solution)/shard_map/psum | solution.py:141
  338.9 3.4 convolution_convert_fusion.2
  342.3 30.8 %all-reduce.10.cloned.1.call-done = bf16[64,512]{1,0:T(8,128)(2,1)} async-done(((bf16[64,512]{1,0:T(8,128)(2,1)}), bf16[64,512]{1,0:T(8,128)(2,1)}) %all-reduce.10.cloned.1.call-update) | async-done | bytes 65552 | tf_op jit(solution)/shard_map/psum | solution.py:147
  (90 shorter events, 30.3 us)
Async XLA Ops:
  6.5 252.3 %copy-start = (bf16[512,2816]{1,0:T(8,128)(2,1)S(1)}, bf16[512,2816]{1,0:T(8,128)(2,1)}, u32[]{:S(2)}) copy-start(bf16[512,2816]{1,0:T(8,128)(2,1)} %param.31) | copy-start | bytes 8650756
  6.5 81.6 %all-reduce.14.cloned.1.call-start = ((), (), s32[]{:S(2)}) async-start(), calls=%async_computation.4 | async-start | bytes 393216 | tf_op jit(solution)/shard_map/psum | solution.py:58
  13.9 191.8 %all-gather.7.cloned.1.call-start = ((), (), s32[]{:S(2)}) async-start(), calls=%async_computation.2 | async-start | bytes 1179648 | tf_op jit(solution)/shard_map/all_gather | solution.py:14
  41.7 48.8 %copy-start.3 = (f32[64]{0:T(128)}, f32[64]{0:T(128)S(1)}, u32[]{:S(2)}) copy-start(f32[64]{0:T(128)S(1)} %add_rsqrt_fusion.1) | copy-start | bytes 772
  90.4 6.5 %copy-start.4 = (bf16[16,512,512]{2,1,0:T(8,128)(2,1)S(1)}, bf16[16,512,512]{2,1,0:T(8,128)(2,1)}, u32[]{:S(2)}) copy-start(bf16[16,512,512]{2,1,0:T(8,128)(2,1)} %param.26) | copy-start | bytes 25165828
  96.3 0.6 copy-start.1
  98.9 158.9 %all-reduce.8.cloned.1.call-start = ((), (), s32[]{:S(2)}) async-start(), calls=%async_computation | async-start | bytes 131072 | tf_op jit(solution)/shard_map/psum | solution.py:130
  131.9 0.6 copy-start.2
  228.5 110.4 %all-reduce.12.cloned.1.call-start = ((), (), s32[]{:S(2)}) async-start(), calls=%async_computation.3 | async-start | bytes 1441792 | tf_op jit(solution)/shard_map/psum | solution.py:141
  264.0 109.1 %all-reduce.10.cloned.1.call-start = ((), (), s32[]{:S(2)}) async-start(), calls=%async_computation.1 | async-start | bytes 131072 | tf_op jit(solution)/shard_map/psum | solution.py:147
Sparse Core Ops, SparseCore 0:
  14.0 74.0 all-reduce.13
  99.0 39.8 all-gather.6
  228.7 29.1 all-reduce.7
  264.2 74.7 all-reduce.11
  342.4 30.6 all-reduce.9
where the time goes:
time: 383 us; the launch traced here: 381 us
  waiting for transfers between devices  160 us (42%)
  blocking collectives  133 us (35%)
  other arithmetic  31.2 us (8%)
  matrix products  26.9 us (7%)
  local copies, waits for them, and re-layouts  16.3 us (4%)
  between operations  13.3 us (3%)
    all_gather x3, blocking collectives, combined_all(): everything = jax.tree.map(lambda part: lax.all_gather(part, axis), array)  88 us
    psum x1, waiting for transfers between devices, on_device(): lax.psum(up_part.astype(jnp.bfloat16), 'kv').astype(jnp.float32)  53.3 us
    psum x1, waiting for transfers between devices, on_device(): lax.psum(query_part.astype(jnp.bfloat16), 'kv').astype(jnp.float32)  46.5 us
    psum x1, waiting for transfers between devices, on_device(): mixed = lax.psum(down_part.astype(jnp.bfloat16), 'tp').astype(jnp.float32)  30.8 us
    psum x1, waiting for transfers between devices, on_device(): lax.psum(jnp.dot(attended, w_out, preferred_element_type=jnp.float32).ast...  29.2 us
    psum x1, blocking collectives, on_device(): lax.psum(squares.astype(jnp.bfloat16), 'kv').astype(jnp.float32)  23.7 us
    psum x1, blocking collectives, on_device(): lax.psum(squares2.astype(jnp.bfloat16), 'kv').astype(jnp.float32)  21.6 us
    add x7, other arithmetic, combine(): first[2] * first_factor[..., None] + second[2] * second_factor[..., None]  9.27 us
  transfers between devices with their start and end apart: 5, of which 4 were waited for; matrix products, arithmetic and copies ran while one was open for 6% of the time, Pallas kernels for 0%

commit v1 on v0

--- a/solution.py
+++ b/solution.py
@@ -1,10 +1,11 @@
 import jax
 import jax.numpy as jnp
+import functools
+
 from jax import lax
+from jax.experimental import pallas as pl
+from jax.experimental.pallas import tpu as pltpu
 from jax.sharding import PartitionSpec as P
-
-D = 4096
-
 
 EPSILON = 1e-06
 NEG_FILL = -1e30
@@ -39,6 +40,7 @@
     w_down,
 ):
     seq_count, new_count, local_width = tokens.shape
+    D = local_width * lax.axis_size("kv")
     row_count = seq_count * new_count
     heads_dev = forget_bias.shape[0]
     head_width = w_query.shape[1] // heads_dev
@@ -148,6 +150,426 @@
     return (middle_wide + mixed).astype(jnp.bfloat16).reshape(seq_count, new_count, local_width)
 
 
+LANES = 128
+MESH = pl.DeviceIdType.MESH
+F32 = jnp.float32
+BF16 = jnp.bfloat16
+
+
+def fused_kernel(
+    n_kv, n_tp, new_count,
+    tok, mix_gain, mlp_gain, bias, lens, wf_h, cum_h, wq_h, wk_h, wv_h,
+    kc_h, vc_h, wo_h, wg_h, wu_h, wd_h,
+    out,
+    wf, cum, wq, wk, wv, kc, vc, wo, wg, wu, wd,
+    sb1, rb1, qb, kn, vn, lf, cs, cr, ab, ap, ar, mid, gs, gr, us, ur, hb, dp, dr,
+    lsem, ksem, vsem, s1, r1, s2, r2, s3, r3, s4, r4, s5, r5, s6, r6, s7, r7, s8, r8, s9, r9,
+):
+    me = lax.axis_index("kv")
+    mt = lax.axis_index("tp")
+    rows, width = tok.shape
+    rp = rows // n_kv
+    sp = rp // new_count
+    heads = bias.shape[0]
+    hw = wq.shape[1]
+    hd = hw // heads
+    pos_dev = kc.shape[1]
+    ff = wg.shape[1]
+    full = width * n_kv
+    scale = hd ** (-0.5)
+
+    def peer(i):
+        return lax.rem(me + i, n_kv)
+
+    def tpeer(i):
+        return lax.rem(mt + i, n_tp)
+
+    loads = [
+        pltpu.make_async_copy(wf_h.at[pl.ds(pl.multiple_of(me * width, width), width)], wf, lsem.at[0]),
+        pltpu.make_async_copy(wq_h, wq, lsem.at[1]),
+        pltpu.make_async_copy(wk_h, wk, lsem.at[2]),
+        pltpu.make_async_copy(wv_h, wv, lsem.at[3]),
+        pltpu.make_async_copy(cum_h, cum, lsem.at[4]),
+        pltpu.make_async_copy(wo_h, wo, lsem.at[5]),
+        pltpu.make_async_copy(wg_h, wg, lsem.at[6]),
+        pltpu.make_async_copy(wu_h, wu, lsem.at[7]),
+        pltpu.make_async_copy(wd_h, wd, lsem.at[8]),
+    ]
+
+    def cache_copies(g):
+        part = pl.ds(g * sp, sp)
+        return (
+            pltpu.make_async_copy(kc_h.at[part], kc.at[part], ksem.at[g]),
+            pltpu.make_async_copy(vc_h.at[part], vc.at[part], vsem.at[g]),
+        )
+
+    for load in loads[:5]:
+        load.start()
+
+    def start_cache(i, c):
+        for copy in cache_copies(peer(i)):
+            copy.start()
+        return c
+
+    lax.fori_loop(0, n_kv, start_cache, 0)
+    for load in loads[5:]:
+        load.start()
+
+    barrier = pltpu.get_barrier_semaphore()
+    for i in range(1, n_kv):
+        pl.semaphore_signal(barrier, inc=1, device_id={"kv": peer(i)}, device_id_type=MESH)
+    for i in range(1, n_tp):
+        pl.semaphore_signal(barrier, inc=1, device_id={"tp": tpeer(i)}, device_id_type=MESH)
+
+    def send_kv(src, dst, send, recv, g):
+        return pltpu.make_async_remote_copy(
+            src_ref=src, dst_ref=dst, send_sem=send, recv_sem=recv,
+            device_id={"kv": g}, device_id_type=MESH,
+        )
+
+    def send_tp(src, dst, send, recv, g):
+        return pltpu.make_async_remote_copy(
+            src_ref=src, dst_ref=dst, send_sem=send, recv_sem=recv,
+            device_id={"tp": g}, device_id_type=MESH,
+        )
+
+    inputs = tok[...].astype(F32)
+    scaled = (inputs * mix_gain[...]).astype(BF16)
+    squares = jnp.sum(inputs * inputs, axis=1, keepdims=True)
+    loads[0].wait()
+    forget_all = jnp.dot(scaled, wf[...], preferred_element_type=F32).astype(BF16)
+    pick_row = lax.broadcasted_iota(jnp.int32, (wf.shape[1], LANES), 0)
+    pick_col = lax.broadcasted_iota(jnp.int32, (wf.shape[1], LANES), 1)
+    pick = jnp.where(
+        (pick_row == pick_col + mt * heads) & (pick_col < heads), 1.0, 0.0
+    ).astype(BF16)
+    forget = jnp.dot(forget_all, pick, preferred_element_type=F32)
+    lane_rows = lax.broadcasted_iota(jnp.int32, (rows, LANES), 1)
+    aux = jnp.where(lane_rows == heads, squares, forget)
+    for g in range(n_kv):
+        sb1[g, :, 3 * hw :] = aux[g * rp : (g + 1) * rp].astype(BF16)
+    for k, (load, weight) in enumerate(zip(loads[1:4], (wq, wk, wv))):
+        load.wait()
+        part = jnp.dot(scaled, weight[...], preferred_element_type=F32)
+        for g in range(n_kv):
+            sb1[g, :, k * hw : (k + 1) * hw] = part[g * rp : (g + 1) * rp].astype(BF16)
+
+    pl.semaphore_wait(barrier, n_kv + n_tp - 2)
+    for i in range(1, n_kv):
+        g = peer(i)
+        send_kv(sb1.at[g], rb1.at[me], s1.at[g], r1.at[me], g).start()
+    total1 = sb1[me].astype(F32)
+    for i in range(1, n_kv):
+        g = peer(i)
+        send_kv(sb1.at[g], rb1.at[g], s1.at[g], r1.at[g], g).wait_recv()
+        total1 = total1 + rb1[g].astype(F32)
+    lane = lax.broadcasted_iota(jnp.int32, (rp, LANES), 1)
+    row8 = lax.broadcasted_iota(jnp.int32, (rp, LANES), 0)
+    aux1 = total1[:, 3 * hw :]
+    inv_norm = lax.rsqrt(aux1[:, heads : heads + 1] / full + EPSILON)
+    qb[me] = (inv_norm * total1[:, :hw]).astype(BF16)
+    for i in range(1, n_kv):
+        g = peer(i)
+        send_kv(qb.at[me], qb.at[me], s2.at[g], r2.at[me], g).start()
+    kn[...] = (inv_norm * total1[:, hw : 2 * hw]).astype(BF16).astype(F32)
+    vn[...] = (inv_norm * total1[:, 2 * hw : 3 * hw]).astype(BF16).astype(F32)
+    bias_row = jnp.zeros((rp, LANES), F32)
+    for h in range(heads):
+        bias_row = jnp.where(lane == h, bias[h], bias_row)
+    logit = inv_norm * aux1 + bias_row
+    lf[...] = -(jnp.maximum(-logit, 0.0) + jnp.log1p(jnp.exp(-jnp.abs(logit))))
+
+    loads[4].wait()
+    col_q = lax.broadcasted_iota(jnp.int32, (rp, hw), 1)
+    row_p = lax.broadcasted_iota(jnp.int32, (rp, pos_dev), 0)
+    pos = me * pos_dev + lax.broadcasted_iota(jnp.int32, (rp, pos_dev), 1)
+
+    def attend(g, dest):
+        q8 = qb[g].astype(F32)
+        spread = jnp.concatenate(
+            [
+                jnp.where((col_q >= h * hd) & (col_q < (h + 1) * hd), q8, 0.0)
+                for h in range(heads)
+            ],
+            axis=0,
+        ).astype(BF16)
+        copy_k, copy_v = cache_copies(g)
+        copy_k.wait()
+        length = jnp.zeros((rp, pos_dev), jnp.int32)
+        products, gates = [], []
+        for j in range(sp):
+            products.append(
+                lax.dot_general(
+                    spread, kc[g * sp + j], (((1,), (1,)), ((), ())), preferred_element_type=F32
+                )
+            )
+            gates.append(cum[g * sp + j])
+            length = jnp.where(row_p >= j * new_count, lens[g * sp + j], length)
+        live = pos < length
+        last_hit = pos == length - 1
+        weight_heads = []
+        extra = jnp.zeros((rp, LANES), F32)
+        for h in range(heads):
+            score, gate = None, None
+            for j in range(sp):
+                score_j = products[j][h * rp : (h + 1) * rp]
+                gate_j = jnp.broadcast_to(gates[j][h : h + 1], (rp, pos_dev))
+                if j == 0:
+                    score, gate = score_j, gate_j
+                else:
+                    score = jnp.where(row_p >= j * new_count, score_j, score)
+                    gate = jnp.where(row_p >= j * new_count, gate_j, gate)
+            score = jnp.where(live, score * scale - gate, NEG_FILL)
+            peak = jnp.max(score, axis=1, keepdims=True)
+            weight = jnp.where(live, jnp.exp(score - peak), 0.0)
+            extra = jnp.where(lane == h, peak, extra)
+            extra = jnp.where(lane == heads + h, jnp.sum(weight, axis=1, keepdims=True), extra)
+            last = jnp.sum(jnp.where(last_hit, gate, 0.0), axis=1, keepdims=True)
+            extra = jnp.where(lane == 2 * heads + h, last, extra)
+            weight_heads.append(weight)
+        weights = jnp.concatenate(weight_heads, axis=0).astype(BF16)
+        copy_v.wait()
+        sums = [
+            jnp.dot(weights, vc[g * sp + j], preferred_element_type=F32) for j in range(sp)
+        ]
+        row_h = row8[:, :1]
+        for h in range(heads):
+            piece = sums[0][h * rp : (h + 1) * rp, h * hd : (h + 1) * hd]
+            for j in range(1, sp):
+                piece_j = sums[j][h * rp : (h + 1) * rp, h * hd : (h + 1) * hd]
+                piece = jnp.where(row_h >= j * new_count, piece_j, piece)
+            dest[:, h * hd : (h + 1) * hd] = piece
+        dest[:, hw:] = extra
+
+    attend(me, cr.at[me])
+
+    def attend_step(i, c):
+        g = peer(i)
+        send_kv(qb.at[me], qb.at[g], s2.at[g], r2.at[g], g).wait_recv()
+        attend(g, cs.at[g])
+        send_kv(cs.at[g], cr.at[me], s3.at[g], r3.at[me], g).start()
+        return c
+
+    lax.fori_loop(1, n_kv, attend_step, 0)
+
+    for i in range(1, n_kv):
+        g = peer(i)
+        send_kv(cs.at[g], cr.at[g], s3.at[g], r3.at[g], g).wait_recv()
+
+    def expand(x):
+        return jnp.concatenate(
+            [jnp.broadcast_to(x[:, h : h + 1], (rp, hd)) for h in range(heads)], axis=1
+        )
+
+    extras = [cr[k, :, hw:] for k in range(n_kv)]
+    past_peak = functools.reduce(jnp.maximum, extras)
+    past_total = jnp.zeros((rp, LANES), F32)
+    last_cum = jnp.zeros((rp, LANES), F32)
+    past_sum = jnp.zeros((rp, hw), F32)
+    for k in range(n_kv):
+        factor = jnp.exp(extras[k] - past_peak)
+        past_total = past_total + pltpu.roll(extras[k], LANES - heads, 1) * factor
+        last_cum = last_cum + pltpu.roll(extras[k], LANES - 2 * heads, 1)
+        past_sum = past_sum + cr[k, :, :hw] * expand(factor)
+
+    def valid(d):
+        hit = (row8 >= d) & (row8 < new_count)
+        for j in range(1, sp):
+            hit = hit | ((row8 >= j * new_count + d) & (row8 < (j + 1) * new_count))
+        return hit
+
+    def shifted(x, d):
+        return x if d == 0 else pltpu.roll(x, d, 0)
+
+    log_forget = lf[...]
+    key_cum = last_cum
+    for d in range(new_count):
+        key_cum = key_cum + jnp.where(valid(d), shifted(log_forget, d), 0.0)
+    own_query = qb[me].astype(F32)
+    own_key, own_value = kn[...], vn[...]
+    own_scores = []
+    for d in range(new_count):
+        product = own_query * shifted(own_key, d)
+        score = jnp.zeros((rp, LANES), F32)
+        for h in range(heads):
+            dot_h = jnp.sum(product[:, h * hd : (h + 1) * hd], axis=1, keepdims=True)
+            score = jnp.where(lane == h, dot_h, score)
+        own_scores.append(
+            jnp.where(valid(d), score * scale - shifted(key_cum, d), NEG_FILL)
+        )
+    peak_score = functools.reduce(jnp.maximum, own_scores, past_peak)
+    past_factor = jnp.exp(past_peak - peak_score)
+    numerator = past_sum * expand(past_factor)
+    denominator = past_total * past_factor
+    for d in range(new_count):
+        own_weight = jnp.where(valid(d), jnp.exp(own_scores[d] - peak_score), 0.0)
+        denominator = denominator + own_weight
+        numerator = numerator + expand(own_weight.astype(BF16).astype(F32)) * shifted(own_value, d)
+    ab[me] = (numerator / expand(denominator)).astype(BF16)
+    for i in range(1, n_kv):
+        g = peer(i)
+        send_kv(ab.at[me], ab.at[me], s4.at[g], r4.at[me], g).start()
+    for i in range(1, n_kv):
+        g = peer(i)
+        send_kv(ab.at[me], ab.at[g], s4.at[g], r4.at[g], g).wait_recv()
+
+    def all_rows(ref):
+        return jnp.concatenate([ref[k].astype(F32) for k in range(n_kv)], axis=0).astype(BF16)
+
+    loads[5].wait()
+    ap[...] = jnp.dot(all_rows(ab), wo[...], preferred_element_type=F32).astype(BF16)
+    for i in range(1, n_tp):
+        g = tpeer(i)
+        send_tp(ap, ar.at[mt], s5.at[g], r5.at[mt], g).start()
+    for i in range(1, n_tp):
+        g = tpeer(i)
+        send_tp(ap, ar.at[g], s5.at[g], r5.at[g], g).wait_recv()
+    attn_out = jnp.zeros((rows, width), F32)
+    for k in range(n_tp):
+        attn_out = attn_out + jnp.where(mt == k, ap[...], ar[k]).astype(F32)
+    middle = (tok[...].astype(F32) + attn_out).astype(BF16)
+    mid[...] = middle
+    wide = middle.astype(F32)
+    squares2 = jnp.sum(wide * wide, axis=1, keepdims=True)
+    scaled2 = (wide * mlp_gain[...]).astype(BF16)
+
+    for g in range(n_kv):
+        gs[g, :, ff:] = jnp.broadcast_to(squares2[g * rp : (g + 1) * rp], (rp, LANES)).astype(BF16)
+    tile = 256 if ff % 256 == 0 else LANES
+    for load, weight, sent, landed, ssem, rsem in (
+        (loads[6], wg, gs, gr, s6, r6),
+        (loads[7], wu, us, ur, s7, r7),
+    ):
+        load.wait()
+
+        def column_tile(c, carry, weight=weight, sent=sent):
+            cols = pl.ds(pl.multiple_of(c * tile, tile), tile)
+            part = jnp.dot(scaled2, weight[:, cols], preferred_element_type=F32)
+            for g in range(n_kv):
+                sent[g, :, cols] = part[g * rp : (g + 1) * rp].astype(BF16)
+            return carry
+
+        lax.fori_loop(0, ff // tile, column_tile, 0)
+        for i in range(1, n_kv):
+            g = peer(i)
+            send_kv(sent.at[g], landed.at[me], ssem.at[g], rsem.at[me], g).start()
+    for i in range(1, n_kv):
+        g = peer(i)
+        send_kv(gs.at[g], gr.at[g], s6.at[g], r6.at[g], g).wait_recv()
+    gate_sum = gs[me].astype(F32)
+    for i in range(1, n_kv):
+        gate_sum = gate_sum + gr[peer(i)].astype(F32)
+    inv_norm2 = lax.rsqrt(gate_sum[:, ff : ff + 1] / full + EPSILON)
+    gate = inv_norm2 * gate_sum[:, :ff]
+    silu = gate / (1.0 + jnp.exp(-gate))
+    for i in range(1, n_kv):
+        g = peer(i)
+        send_kv(us.at[g], ur.at[g], s7.at[g], r7.at[g], g).wait_recv()
+    up_sum = us[me].astype(F32)
+    for i in range(1, n_kv):
+        up_sum = up_sum + ur[peer(i)].astype(F32)
+    hb[me] = (silu * (inv_norm2 * up_sum)).astype(BF16)
+    for i in range(1, n_kv):
+        g = peer(i)
+        send_kv(hb.at[me], hb.at[me], s8.at[g], r8.at[me], g).start()
+    for i in range(1, n_kv):
+        g = peer(i)
+        send_kv(hb.at[me], hb.at[g], s8.at[g], r8.at[g], g).wait_recv()
+
+    loads[8].wait()
+    dp[...] = jnp.dot(all_rows(hb), wd[...], preferred_element_type=F32).astype(BF16)
+    for i in range(1, n_tp):
+        g = tpeer(i)
+        send_tp(dp, dr.at[mt], s9.at[g], r9.at[mt], g).start()
+    for i in range(1, n_tp):
+        g = tpeer(i)
+        send_tp(dp, dr.at[g], s9.at[g], r9.at[g], g).wait_recv()
+    mixed = jnp.zeros((rows, width), F32)
+    for k in range(n_tp):
+        mixed = mixed + jnp.where(mt == k, dp[...], dr[k]).astype(F32)
+    out[...] = (mid[...].astype(F32) + mixed).astype(BF16)
+
+    for i in range(1, n_kv):
+        g = peer(i)
+        send_kv(sb1.at[g], rb1.at[me], s1.at[g], r1.at[me], g).wait_send()
+        send_kv(qb.at[me], qb.at[me], s2.at[g], r2.at[me], g).wait_send()
+        send_kv(cs.at[g], cr.at[me], s3.at[g], r3.at[me], g).wait_send()
+        send_kv(ab.at[me], ab.at[me], s4.at[g], r4.at[me], g).wait_send()
+        send_kv(gs.at[g], gr.at[me], s6.at[g], r6.at[me], g).wait_send()
+        send_kv(us.at[g], ur.at[me], s7.at[g], r7.at[me], g).wait_send()
+        send_kv(hb.at[me], hb.at[me], s8.at[g], r8.at[me], g).wait_send()
+    for i in range(1, n_tp):
+        g = tpeer(i)
+        send_tp(ap, ar.at[mt], s5.at[g], r5.at[mt], g).wait_send()
+        send_tp(dp, dr.at[mt], s9.at[g], r9.at[mt], g).wait_send()
+
+
+def fused_on_device(
+    tokens, mix_gain, w_query, w_key, w_value, w_forget, forget_bias, key_cache, value_cache,
+    cum_gate, lengths, w_out, mlp_gain, w_gate, w_up, w_down,
+):
+    n_kv, n_tp = lax.axis_size("kv"), lax.axis_size("tp")
+    seq_count, new_count, width = tokens.shape
+    rows = seq_count * new_count
+    rp = rows // n_kv
+    hw = w_query.shape[1]
+    ff = w_gate.shape[1]
+    vmem = pl.BlockSpec(memory_space=pltpu.VMEM)
+    smem = pl.BlockSpec(memory_space=pltpu.SMEM)
+    anywhere = pl.BlockSpec(memory_space=pl.ANY)
+    kv_sems = pltpu.SemaphoreType.DMA((n_kv,))
+    tp_sems = pltpu.SemaphoreType.DMA((n_tp,))
+
+    def like(x):
+        return pltpu.VMEM(x.shape, x.dtype)
+
+    result = pl.pallas_call(
+        functools.partial(fused_kernel, n_kv, n_tp, new_count),
+        out_shape=jax.ShapeDtypeStruct((rows, width), BF16),
+        in_specs=[vmem] * 3 + [smem] * 2 + [anywhere] * 11,
+        out_specs=vmem,
+        scratch_shapes=[
+            pltpu.VMEM((width, w_forget.shape[1]), BF16),
+            like(cum_gate), like(w_query), like(w_key), like(w_value),
+            like(key_cache), like(value_cache), like(w_out), like(w_gate), like(w_up),
+            like(w_down),
+            pltpu.VMEM((n_kv, rp, 3 * hw + LANES), BF16),
+            pltpu.VMEM((n_kv, rp, 3 * hw + LANES), BF16),
+            pltpu.VMEM((n_kv, rp, hw), BF16),
+            pltpu.VMEM((rp, hw), F32),
+            pltpu.VMEM((rp, hw), F32),
+            pltpu.VMEM((rp, LANES), F32),
+            pltpu.VMEM((n_kv, rp, hw + LANES), F32),
+            pltpu.VMEM((n_kv, rp, hw + LANES), F32),
+            pltpu.VMEM((n_kv, rp, hw), BF16),
+            pltpu.VMEM((rows, width), BF16),
+            pltpu.VMEM((n_tp, rows, width), BF16),
+            pltpu.VMEM((rows, width), BF16),
+            pltpu.VMEM((n_kv, rp, ff + LANES), BF16),
+            pltpu.VMEM((n_kv, rp, ff + LANES), BF16),
+            pltpu.VMEM((n_kv, rp, ff), BF16),
+            pltpu.VMEM((n_kv, rp, ff), BF16),
+            pltpu.VMEM((n_kv, rp, ff), BF16),
+            pltpu.VMEM((rows, width), BF16),
+            pltpu.VMEM((n_tp, rows, width), BF16),
+            pltpu.SemaphoreType.DMA((9,)),
+            kv_sems, kv_sems,
+            kv_sems, kv_sems, kv_sems, kv_sems, kv_sems, kv_sems, kv_sems, kv_sems,
+            tp_sems, tp_sems,
+            kv_sems, kv_sems, kv_sems, kv_sems, kv_sems, kv_sems,
+            tp_sems, tp_sems,
+        ],
+        compiler_params=pltpu.CompilerParams(
+            collective_id=0, has_side_effects=True, vmem_limit_bytes=60 * 1024 * 1024
+        ),
+    )(
+        tokens.reshape(rows, width), mix_gain.reshape(1, width), mlp_gain.reshape(1, width),
+        forget_bias, lengths, w_forget, cum_gate, w_query, w_key, w_value,
+        key_cache, value_cache, w_out, w_gate, w_up, w_down,
+    )
+    return result.reshape(seq_count, new_count, width)
+
+
 def solution(mesh):
     in_specs = (
         P(None, None, "kv"),
@@ -168,6 +590,14 @@
         P("tp", "kv"),
     )
     out_specs = P(None, None, "kv")
+
+    def layer(*arrays):
+        seq_count, new_count, _ = arrays[0].shape
+        rows_kv, rest = divmod(seq_count * new_count, jax.lax.axis_size("kv"))
+        if rest or rows_kv % 8 or rows_kv % new_count:
+            return on_device(*arrays)
+        return fused_on_device(*arrays)
+
     return jax.shard_map(
-        on_device, mesh=mesh, in_specs=in_specs, out_specs=out_specs, check_vma=False
-    )
+        layer, mesh=mesh, in_specs=in_specs, out_specs=out_specs, check_vma=False
+    )

time: 383 us -> 72.7 us (0.19)
  the two profiles are of different devices: /device:TPU:0 before, /device:TPU:25 now
where the time goes in v1:
time: 72.7 us; the launch traced here: 72.5 us
  Pallas kernels  67.3 us (93%)
  local copies, waits for them, and re-layouts  5.22 us (7%)
    pallas_call x1, Pallas kernels, fused_on_device(): pl.pallas_call(functools.partial(fused_kernel, n_kv, n_tp, new_count), ou...  67.3 us
    unnamed x1, local copies, waits for them, and re-layouts  2.24 us
    reshape x1, local copies, waits for them, and re-layouts, fused_on_device(): return result.reshape(seq_count, new_count, width)  1.49 us
    reshape x1, local copies, waits for them, and re-layouts, fused_on_device(): tokens.reshape(rows, width)  1.49 us

profile of v1, /device:TPU:25, one launch (start us, length us, event | category | flops | bytes accessed | tf_op | source)
XLA Modules:
  0.0 72.5 jit_solution(7347359483549884881)
XLA Ops:
  0.0 1.5 %reshape.12.tok = bf16[64,512]{1,0:T(8,128)(2,1)} reshape(bf16[16,4,512]{2,1,0:T(4,128)(2,1)} %param.16) | data formatting | bytes 131072 | tf_op jit(solution)/shard_map/reshape | solution.py:566
  1.5 2.2 %copy.17.wf_h = bf16[4096,16]{1,0:T(8,128)(2,1)} copy(bf16[4096,16]{0,1:T(8,128)(2,1)} %param.21) | data formatting | bytes 262144 | tf_op args[5]
  3.7 67.3 %shard_map.154 = bf16[64,512]{1,0:T(8,128)(2,1)} custom-call(bf16[64,512]{1,0:T(8,128)(2,1)} %reshape.12.tok, f32[1,512]{1,0:T(1,128)} %bitcast.2, f32[1,512]{1,0:T(1,128)} %bitcast.3, f32[4]{0:T(128)} %bias.1, s32[16]{0:T(128)} %lens.1, bf16[4096,16]{1,0:T(8,128)(2,1)} %copy.17.wf_h, f32[16,4,512]{2,1,0:T(4,128)} %cum_h.1, bf16[512,512]{1,0:T(8,128)(2,1)} %wq_h.1, ...), custom_call_target="tpu_custom_call" | custom-call | tf_op jit(solution)/shard_map/pallas_call | solution.py:526
  71.0 1.5 %reshape.15 = bf16[16,4,512]{2,1,0:T(4,128)(2,1)} reshape(bf16[64,512]{1,0:T(8,128)(2,1)} %shard_map.154) | data formatting | bytes 131072 | tf_op jit(solution)/shard_map/reshape | solution.py:570

commit v2 on v1

--- a/solution.py
+++ b/solution.py
@@ -158,12 +158,13 @@
 
 def fused_kernel(
     n_kv, n_tp, new_count,
-    tok, mix_gain, mlp_gain, bias, lens, wf_h, cum_h, wq_h, wk_h, wv_h,
+    tok_h, mix_gain, mlp_gain, bias, lens, wf_h, cum_h, wq_h, wk_h, wv_h,
     kc_h, vc_h, wo_h, wg_h, wu_h, wd_h,
     out,
     wf, cum, wq, wk, wv, kc, vc, wo, wg, wu, wd,
-    sb1, rb1, qb, kn, vn, lf, cs, cr, ab, ap, ar, mid, gs, gr, us, ur, hb, dp, dr,
+    sb1, rb1, sb2, rb2, qb, inv_keep, lf, cs, cr, ab, ap, ar, mid, gs, gy, gf, gr, us, uy, uf, ur, ha, hb, dp, dr,
     lsem, ksem, vsem, s1, r1, s2, r2, s3, r3, s4, r4, s5, r5, s6, r6, s7, r7, s8, r8, s9, r9,
+    s10, r10, s11, r11, s12, r12, s13, s14, r14, s15, tok, tok_blocks,
 ):
     me = lax.axis_index("kv")
     mt = lax.axis_index("tp")
@@ -175,9 +176,14 @@
     hd = hw // heads
     pos_dev = kc.shape[1]
     ff = wg.shape[1]
+    first_width = ha.shape[2]
     full = width * n_kv
     scale = hd ** (-0.5)
 
+    pairs = n_kv // 2
+    z, y = lax.div(me, 2), lax.rem(me, 2)
+    mate = 2 * z + 1 - y
+
     def peer(i):
         return lax.rem(me + i, n_kv)
 
@@ -185,7 +191,7 @@
         return lax.rem(mt + i, n_tp)
 
     loads = [
-        pltpu.make_async_copy(wf_h.at[pl.ds(pl.multiple_of(me * width, width), width)], wf, lsem.at[0]),
+        pltpu.make_async_copy(wf_h.at[:, pl.ds(pl.multiple_of(me * width, width), width)], wf, lsem.at[0]),
         pltpu.make_async_copy(wq_h, wq, lsem.at[1]),
         pltpu.make_async_copy(wk_h, wk, lsem.at[2]),
         pltpu.make_async_copy(wv_h, wv, lsem.at[3]),
@@ -203,6 +209,8 @@
             pltpu.make_async_copy(vc_h.at[part], vc.at[part], vsem.at[g]),
         )
 
+    tok_load = pltpu.make_async_copy(tok_h, tok_blocks, lsem.at[9])
+    tok_load.start()
     for load in loads[:5]:
         load.start()
 
@@ -233,13 +241,18 @@
             device_id={"tp": g}, device_id_type=MESH,
         )
 
-    inputs = tok[...].astype(F32)
+    tok_load.wait()
+    for b in range(tok_blocks.shape[0]):
+        tok[b * new_count : (b + 1) * new_count] = tok_blocks[b].astype(F32)
+    inputs = tok[...]
     scaled = (inputs * mix_gain[...]).astype(BF16)
     squares = jnp.sum(inputs * inputs, axis=1, keepdims=True)
     loads[0].wait()
-    forget_all = jnp.dot(scaled, wf[...], preferred_element_type=F32).astype(BF16)
-    pick_row = lax.broadcasted_iota(jnp.int32, (wf.shape[1], LANES), 0)
-    pick_col = lax.broadcasted_iota(jnp.int32, (wf.shape[1], LANES), 1)
+    forget_all = lax.dot_general(
+        scaled, wf[...], (((1,), (1,)), ((), ())), preferred_element_type=F32
+    ).astype(BF16)
+    pick_row = lax.broadcasted_iota(jnp.int32, (wf.shape[0], LANES), 0)
+    pick_col = lax.broadcasted_iota(jnp.int32, (wf.shape[0], LANES), 1)
     pick = jnp.where(
         (pick_row == pick_col + mt * heads) & (pick_col < heads), 1.0, 0.0
     ).astype(BF16)
@@ -247,17 +260,21 @@
     lane_rows = lax.broadcasted_iota(jnp.int32, (rows, LANES), 1)
     aux = jnp.where(lane_rows == heads, squares, forget)
     for g in range(n_kv):
-        sb1[g, :, 3 * hw :] = aux[g * rp : (g + 1) * rp].astype(BF16)
-    for k, (load, weight) in enumerate(zip(loads[1:4], (wq, wk, wv))):
+        sb1[g, :, hw:] = aux[g * rp : (g + 1) * rp].astype(BF16)
+
+    def project(load, weight, dest, first):
         load.wait()
         part = jnp.dot(scaled, weight[...], preferred_element_type=F32)
         for g in range(n_kv):
-            sb1[g, :, k * hw : (k + 1) * hw] = part[g * rp : (g + 1) * rp].astype(BF16)
-
+            dest[g, :, first : first + hw] = part[g * rp : (g + 1) * rp].astype(BF16)
+
+    project(loads[1], wq, sb1, 0)
     pl.semaphore_wait(barrier, n_kv + n_tp - 2)
     for i in range(1, n_kv):
         g = peer(i)
         send_kv(sb1.at[g], rb1.at[me], s1.at[g], r1.at[me], g).start()
+    project(loads[2], wk, sb2, 0)
+    project(loads[3], wv, sb2, hw)
     total1 = sb1[me].astype(F32)
     for i in range(1, n_kv):
         g = peer(i)
@@ -265,19 +282,21 @@
         total1 = total1 + rb1[g].astype(F32)
     lane = lax.broadcasted_iota(jnp.int32, (rp, LANES), 1)
     row8 = lax.broadcasted_iota(jnp.int32, (rp, LANES), 0)
-    aux1 = total1[:, 3 * hw :]
+    aux1 = total1[:, hw:]
     inv_norm = lax.rsqrt(aux1[:, heads : heads + 1] / full + EPSILON)
     qb[me] = (inv_norm * total1[:, :hw]).astype(BF16)
     for i in range(1, n_kv):
         g = peer(i)
         send_kv(qb.at[me], qb.at[me], s2.at[g], r2.at[me], g).start()
-    kn[...] = (inv_norm * total1[:, hw : 2 * hw]).astype(BF16).astype(F32)
-    vn[...] = (inv_norm * total1[:, 2 * hw : 3 * hw]).astype(BF16).astype(F32)
+    for i in range(1, n_kv):
+        g = peer(i)
+        send_kv(sb2.at[g], rb2.at[me], s10.at[g], r10.at[me], g).start()
     bias_row = jnp.zeros((rp, LANES), F32)
     for h in range(heads):
         bias_row = jnp.where(lane == h, bias[h], bias_row)
     logit = inv_norm * aux1 + bias_row
     lf[...] = -(jnp.maximum(-logit, 0.0) + jnp.log1p(jnp.exp(-jnp.abs(logit))))
+    inv_keep[...] = jnp.broadcast_to(inv_norm, (rp, LANES))
 
     loads[4].wait()
     col_q = lax.broadcasted_iota(jnp.int32, (rp, hw), 1)
@@ -352,6 +371,14 @@
 
     lax.fori_loop(1, n_kv, attend_step, 0)
 
+    total2 = sb2[me].astype(F32)
+    for i in range(1, n_kv):
+        g = peer(i)
+        send_kv(sb2.at[g], rb2.at[g], s10.at[g], r10.at[g], g).wait_recv()
+        total2 = total2 + rb2[g].astype(F32)
+    own_scale = inv_keep[:, :1]
+    own_key = (own_scale * total2[:, :hw]).astype(BF16).astype(F32)
+    own_value = (own_scale * total2[:, hw:]).astype(BF16).astype(F32)
     for i in range(1, n_kv):
         g = peer(i)
         send_kv(cs.at[g], cr.at[g], s3.at[g], r3.at[g], g).wait_recv()
@@ -386,7 +413,6 @@
     for d in range(new_count):
         key_cum = key_cum + jnp.where(valid(d), shifted(log_forget, d), 0.0)
     own_query = qb[me].astype(F32)
-    own_key, own_value = kn[...], vn[...]
     own_scores = []
     for d in range(new_count):
         product = own_query * shifted(own_key, d)
@@ -427,57 +453,104 @@
     attn_out = jnp.zeros((rows, width), F32)
     for k in range(n_tp):
         attn_out = attn_out + jnp.where(mt == k, ap[...], ar[k]).astype(F32)
-    middle = (tok[...].astype(F32) + attn_out).astype(BF16)
+    middle = (tok[...] + attn_out).astype(BF16)
     mid[...] = middle
     wide = middle.astype(F32)
     squares2 = jnp.sum(wide * wide, axis=1, keepdims=True)
     scaled2 = (wide * mlp_gain[...]).astype(BF16)
 
     for g in range(n_kv):
-        gs[g, :, ff:] = jnp.broadcast_to(squares2[g * rp : (g + 1) * rp], (rp, LANES)).astype(BF16)
-    tile = 256 if ff % 256 == 0 else LANES
-    for load, weight, sent, landed, ssem, rsem in (
-        (loads[6], wg, gs, gr, s6, r6),
-        (loads[7], wu, us, ur, s7, r7),
+        gs[g, :, 2 * first_width :] = jnp.broadcast_to(
+            squares2[g * rp : (g + 1) * rp], (rp, LANES)
+        ).astype(BF16)
+    tile = 256 if ff % 256 == 0 and first_width % 256 == 0 else LANES
+    loads[6].wait()
+    loads[7].wait()
+    for start, span, sent, landed, ssem, rsem in (
+        (0, first_width, gs, gy, s6, r6),
+        (first_width, ff - first_width, us, uy, s7, r7),
     ):
-        load.wait()
-
-        def column_tile(c, carry, weight=weight, sent=sent):
-            cols = pl.ds(pl.multiple_of(c * tile, tile), tile)
-            part = jnp.dot(scaled2, weight[:, cols], preferred_element_type=F32)
-            for g in range(n_kv):
-                sent[g, :, cols] = part[g * rp : (g + 1) * rp].astype(BF16)
-            return carry
-
-        lax.fori_loop(0, ff // tile, column_tile, 0)
-        for i in range(1, n_kv):
-            g = peer(i)
-            send_kv(sent.at[g], landed.at[me], ssem.at[g], rsem.at[me], g).start()
-    for i in range(1, n_kv):
-        g = peer(i)
-        send_kv(gs.at[g], gr.at[g], s6.at[g], r6.at[g], g).wait_recv()
-    gate_sum = gs[me].astype(F32)
-    for i in range(1, n_kv):
-        gate_sum = gate_sum + gr[peer(i)].astype(F32)
-    inv_norm2 = lax.rsqrt(gate_sum[:, ff : ff + 1] / full + EPSILON)
-    gate = inv_norm2 * gate_sum[:, :ff]
-    silu = gate / (1.0 + jnp.exp(-gate))
-    for i in range(1, n_kv):
-        g = peer(i)
-        send_kv(us.at[g], ur.at[g], s7.at[g], r7.at[g], g).wait_recv()
-    up_sum = us[me].astype(F32)
-    for i in range(1, n_kv):
-        up_sum = up_sum + ur[peer(i)].astype(F32)
-    hb[me] = (silu * (inv_norm2 * up_sum)).astype(BF16)
-    for i in range(1, n_kv):
-        g = peer(i)
-        send_kv(hb.at[me], hb.at[me], s8.at[g], r8.at[me], g).start()
-    for i in range(1, n_kv):
-        g = peer(i)
-        send_kv(hb.at[me], hb.at[g], s8.at[g], r8.at[g], g).wait_recv()
+        for offset, weight in ((0, wg), (span, wu)):
+
+            def column_tile(
+                c, carry, start=start, offset=offset, weight=weight, sent=sent
+            ):
+                cols = pl.ds(pl.multiple_of(start + c * tile, tile), tile)
+                part = jnp.dot(scaled2, weight[:, cols], preferred_element_type=F32)
+                place = pl.ds(pl.multiple_of(offset + c * tile, tile), tile)
+                for g in range(n_kv):
+                    sent[g, :, place] = part[g * rp : (g + 1) * rp].astype(BF16)
+                return carry
+
+            lax.fori_loop(0, span // tile, column_tile, 0)
+        for i in range(1, pairs + 1):
+            zz = lax.rem(z + i, pairs)
+            send_kv(sent.at[2 * zz + 1 - y], landed.at[zz], ssem.at[zz], rsem.at[zz], mate).start()
+
+    def second_hop(sent, landed, forward, arrived, ssem, rsem, ssem2, rsem2):
+        for i in range(1, pairs + 1):
+            zz = lax.rem(z + i, pairs)
+            send_kv(sent.at[2 * zz + 1 - y], landed.at[zz], ssem.at[zz], rsem.at[zz], mate).wait_recv()
+            both = sent[2 * zz + y].astype(F32) + landed[zz].astype(F32)
+            if i == pairs:
+                return both
+            forward[zz] = both.astype(BF16)
+            send_kv(
+                forward.at[zz], arrived.at[z], ssem2.at[zz], rsem2.at[z], 2 * zz + y
+            ).start()
+
+    def finish_sum(both, forward, arrived, ssem2, rsem2):
+        for i in range(1, pairs):
+            zz = lax.rem(z + i, pairs)
+            send_kv(
+                forward.at[zz], arrived.at[zz], ssem2.at[zz], rsem2.at[zz], 2 * zz + y
+            ).wait_recv()
+            both = both + arrived[zz].astype(F32)
+        return both
+
+    def gather_start(block, ssem, msem, rsem):
+        for i in range(1, pairs):
+            zz = lax.rem(z + i, pairs)
+            send_kv(block.at[me], block.at[me], ssem.at[zz], rsem.at[me], 2 * zz + y).start()
+        send_kv(block.at[me], block.at[me], msem.at[z], rsem.at[me], mate).start()
+
+    def gather_forward(block, ssem, msem, rsem):
+        for i in range(1, pairs):
+            zz = lax.rem(z + i, pairs)
+            slot = 2 * zz + y
+            send_kv(block.at[me], block.at[slot], ssem.at[zz], rsem.at[slot], slot).wait_recv()
+            send_kv(block.at[slot], block.at[slot], msem.at[zz], rsem.at[slot], mate).start()
+
+    def gather_end(block, msem, rsem):
+        for i in range(1, pairs + 1):
+            zz = lax.rem(z + i, pairs)
+            slot = 2 * zz + 1 - y
+            send_kv(block.at[me], block.at[slot], msem.at[zz], rsem.at[slot], mate).wait_recv()
+
+    def gated(total, span):
+        gate = inv_norm2 * total[:, :span]
+        return (gate / (1.0 + jnp.exp(-gate)) * (inv_norm2 * total[:, span : 2 * span])).astype(BF16)
+
+    first_both = second_hop(gs, gy, gf, gr, s6, r6, s11, r11)
+    second_both = second_hop(us, uy, uf, ur, s7, r7, s12, r12)
+    first_sum = finish_sum(first_both, gf, gr, s11, r11)
+    inv_norm2 = lax.rsqrt(
+        first_sum[:, 2 * first_width : 2 * first_width + 1] / full + EPSILON
+    )
+    ha[me] = gated(first_sum, first_width)
+    gather_start(ha, s8, s13, r8)
+    second_sum = finish_sum(second_both, uf, ur, s12, r12)
+    hb[me] = gated(second_sum, ff - first_width)
+    gather_start(hb, s14, s15, r14)
+    gather_forward(ha, s8, s13, r8)
+    gather_forward(hb, s14, s15, r14)
+    gather_end(ha, s13, r8)
 
     loads[8].wait()
-    dp[...] = jnp.dot(all_rows(hb), wd[...], preferred_element_type=F32).astype(BF16)
+    down = jnp.dot(all_rows(ha), wd[:first_width], preferred_element_type=F32)
+    gather_end(hb, s15, r14)
+    down = down + jnp.dot(all_rows(hb), wd[first_width:], preferred_element_type=F32)
+    dp[...] = down.astype(BF16)
     for i in range(1, n_tp):
         g = tpeer(i)
         send_tp(dp, dr.at[mt], s9.at[g], r9.at[mt], g).start()
@@ -495,9 +568,19 @@
         send_kv(qb.at[me], qb.at[me], s2.at[g], r2.at[me], g).wait_send()
         send_kv(cs.at[g], cr.at[me], s3.at[g], r3.at[me], g).wait_send()
         send_kv(ab.at[me], ab.at[me], s4.at[g], r4.at[me], g).wait_send()
-        send_kv(gs.at[g], gr.at[me], s6.at[g], r6.at[me], g).wait_send()
-        send_kv(us.at[g], ur.at[me], s7.at[g], r7.at[me], g).wait_send()
-        send_kv(hb.at[me], hb.at[me], s8.at[g], r8.at[me], g).wait_send()
+        send_kv(sb2.at[g], rb2.at[me], s10.at[g], r10.at[me], g).wait_send()
+    for zz in range(pairs):
+        send_kv(gs.at[0], gy.at[zz], s6.at[zz], r6.at[zz], mate).wait_send()
+        send_kv(us.at[0], uy.at[zz], s7.at[zz], r7.at[zz], mate).wait_send()
+        send_kv(ha.at[me], ha.at[me], s13.at[zz], r8.at[me], mate).wait_send()
+        send_kv(hb.at[me], hb.at[me], s15.at[zz], r14.at[me], mate).wait_send()
+    for i in range(1, pairs):
+        zz = lax.rem(z + i, pairs)
+        g = 2 * zz + y
+        send_kv(gf.at[zz], gr.at[z], s11.at[zz], r11.at[z], g).wait_send()
+        send_kv(uf.at[zz], ur.at[z], s12.at[zz], r12.at[z], g).wait_send()
+        send_kv(ha.at[me], ha.at[me], s8.at[zz], r8.at[me], g).wait_send()
+        send_kv(hb.at[me], hb.at[me], s14.at[zz], r14.at[me], g).wait_send()
     for i in range(1, n_tp):
         g = tpeer(i)
         send_tp(ap, ar.at[mt], s5.at[g], r5.at[mt], g).wait_send()
@@ -514,6 +597,7 @@
     rp = rows // n_kv
     hw = w_query.shape[1]
     ff = w_gate.shape[1]
+    first_width = -(-ff // 512) * 256
     vmem = pl.BlockSpec(memory_space=pltpu.VMEM)
     smem = pl.BlockSpec(memory_space=pltpu.SMEM)
     anywhere = pl.BlockSpec(memory_space=pl.ANY)
@@ -526,18 +610,19 @@
     result = pl.pallas_call(
         functools.partial(fused_kernel, n_kv, n_tp, new_count),
         out_shape=jax.ShapeDtypeStruct((rows, width), BF16),
-        in_specs=[vmem] * 3 + [smem] * 2 + [anywhere] * 11,
+        in_specs=[anywhere] + [vmem] * 2 + [smem] * 2 + [anywhere] * 11,
         out_specs=vmem,
         scratch_shapes=[
-            pltpu.VMEM((width, w_forget.shape[1]), BF16),
+            pltpu.VMEM((w_forget.shape[1], width), BF16),
             like(cum_gate), like(w_query), like(w_key), like(w_value),
             like(key_cache), like(value_cache), like(w_out), like(w_gate), like(w_up),
             like(w_down),
-            pltpu.VMEM((n_kv, rp, 3 * hw + LANES), BF16),
-            pltpu.VMEM((n_kv, rp, 3 * hw + LANES), BF16),
+            pltpu.VMEM((n_kv, rp, hw + LANES), BF16),
+            pltpu.VMEM((n_kv, rp, hw + LANES), BF16),
+            pltpu.VMEM((n_kv, rp, 2 * hw), BF16),
+            pltpu.VMEM((n_kv, rp, 2 * hw), BF16),
             pltpu.VMEM((n_kv, rp, hw), BF16),
-            pltpu.VMEM((rp, hw), F32),
-            pltpu.VMEM((rp, hw), F32),
+            pltpu.VMEM((rp, LANES), F32),
             pltpu.VMEM((rp, LANES), F32),
             pltpu.VMEM((n_kv, rp, hw + LANES), F32),
             pltpu.VMEM((n_kv, rp, hw + LANES), F32),
@@ -545,26 +630,35 @@
             pltpu.VMEM((rows, width), BF16),
             pltpu.VMEM((n_tp, rows, width), BF16),
             pltpu.VMEM((rows, width), BF16),
-            pltpu.VMEM((n_kv, rp, ff + LANES), BF16),
-            pltpu.VMEM((n_kv, rp, ff + LANES), BF16),
-            pltpu.VMEM((n_kv, rp, ff), BF16),
-            pltpu.VMEM((n_kv, rp, ff), BF16),
-            pltpu.VMEM((n_kv, rp, ff), BF16),
+            pltpu.VMEM((n_kv, rp, 2 * first_width + LANES), BF16),
+            pltpu.VMEM((n_kv // 2, rp, 2 * first_width + LANES), BF16),
+            pltpu.VMEM((n_kv // 2, rp, 2 * first_width + LANES), BF16),
+            pltpu.VMEM((n_kv // 2, rp, 2 * first_width + LANES), BF16),
+            pltpu.VMEM((n_kv, rp, 2 * (ff - first_width)), BF16),
+            pltpu.VMEM((n_kv // 2, rp, 2 * (ff - first_width)), BF16),
+            pltpu.VMEM((n_kv // 2, rp, 2 * (ff - first_width)), BF16),
+            pltpu.VMEM((n_kv // 2, rp, 2 * (ff - first_width)), BF16),
+            pltpu.VMEM((n_kv, rp, first_width), BF16),
+            pltpu.VMEM((n_kv, rp, ff - first_width), BF16),
             pltpu.VMEM((rows, width), BF16),
             pltpu.VMEM((n_tp, rows, width), BF16),
-            pltpu.SemaphoreType.DMA((9,)),
+            pltpu.SemaphoreType.DMA((10,)),
             kv_sems, kv_sems,
             kv_sems, kv_sems, kv_sems, kv_sems, kv_sems, kv_sems, kv_sems, kv_sems,
             tp_sems, tp_sems,
             kv_sems, kv_sems, kv_sems, kv_sems, kv_sems, kv_sems,
             tp_sems, tp_sems,
+            kv_sems, kv_sems, kv_sems, kv_sems, kv_sems, kv_sems, kv_sems,
+            kv_sems, kv_sems, kv_sems,
+            pltpu.VMEM((rows, width), F32),
+            like(tokens),
         ],
         compiler_params=pltpu.CompilerParams(
             collective_id=0, has_side_effects=True, vmem_limit_bytes=60 * 1024 * 1024
         ),
     )(
-        tokens.reshape(rows, width), mix_gain.reshape(1, width), mlp_gain.reshape(1, width),
-        forget_bias, lengths, w_forget, cum_gate, w_query, w_key, w_value,
+        tokens, mix_gain.reshape(1, width), mlp_gain.reshape(1, width),
+        forget_bias, lengths, w_forget.T, cum_gate, w_query, w_key, w_value,
         key_cache, value_cache, w_out, w_gate, w_up, w_down,
     )
     return result.reshape(seq_count, new_count, width)
@@ -594,7 +688,7 @@
     def layer(*arrays):
         seq_count, new_count, _ = arrays[0].shape
         rows_kv, rest = divmod(seq_count * new_count, jax.lax.axis_size("kv"))
-        if rest or rows_kv % 8 or rows_kv % new_count:
+        if rest or rows_kv % 8 or rows_kv % new_count or jax.lax.axis_size("kv") % 2:
             return on_device(*arrays)
         return fused_on_device(*arrays)
 

time: 72.7 us -> 63.6 us (0.87)
  the two profiles are of different devices: /device:TPU:25 before, /device:TPU:0 now
where the time goes in v2:
time: 63.6 us; the launch traced here: 63.4 us
  Pallas kernels  61.9 us (97%)
  local copies, waits for them, and re-layouts  1.49 us (2%)
    pallas_call x1, Pallas kernels, fused_on_device(): pl.pallas_call(functools.partial(fused_kernel, n_kv, n_tp, new_count), ou...  61.9 us
    reshape x1, local copies, waits for them, and re-layouts, fused_on_device(): return result.reshape(seq_count, new_count, width)  1.49 us

profile of v2, /device:TPU:0, one launch (start us, length us, event | category | flops | bytes accessed | tf_op | source)
XLA Modules:
  0.0 63.4 jit_solution(13673858959301789701)
XLA Ops:
  0.0 61.9 %shard_map.154 = bf16[64,512]{1,0:T(8,128)(2,1)} custom-call(bf16[16,4,512]{2,1,0:T(4,128)(2,1)} %tok_h.1, f32[1,512]{1,0:T(1,128)} %bitcast.4, f32[1,512]{1,0:T(1,128)} %bitcast.5, f32[4]{0:T(128)} %bias.1, s32[16]{0:T(128)} %lens.1, bf16[16,4096]{1,0:T(8,128)(2,1)} %bitcast.3, f32[16,4,512]{2,1,0:T(4,128)} %cum_h.1, bf16[512,512]{1,0:T(8,128)(2,1)} %wq_h.1, ...), custom_call_target="tpu_custom_call" | custom-call | tf_op jit(solution)/shard_map/pallas_call | solution.py:610
  61.9 1.5 %reshape.11 = bf16[16,4,512]{2,1,0:T(4,128)(2,1)} reshape(bf16[64,512]{1,0:T(8,128)(2,1)} %shard_map.154) | data formatting | bytes 131072 | tf_op jit(solution)/shard_map/reshape | solution.py:664
